TPU v7x, 128 devices: a whole 4x4x4 slice. The times are simulated.
128 devices in a mesh: row: 16 (over z, x), col: 8 (over y, core).
Axes of the slice: x: 4, y: 4, z: 4, core: 2. Of those that a mesh axis runs over, the one named last changes fastest.
Arguments:
- tokens: bfloat16 [65536, 4096], P(('row', 'col')), may hold values from -36 to 36
- norm_gain: bfloat16 [4096], replicated, may hold values from 0.099609375 to 1.8984375
- in_weight: bfloat16 [4096, 1024], replicated, may hold values from -0.09375 to 0.09375
- out_weight: bfloat16 [1024, 4096], replicated, may hold values from -0.1875 to 0.1875
Outputs:
- mixed: bfloat16 [65536, 4096], P(('row', 'col'))
All inputs are finite; a program needn't handle non-finite values.
Results may differ from a plain program's by a relative error of at most 0.0071.
Values may be sent and summed in bfloat16 or wider, within the bound.
A program may use at most 128 MiB of HBM per device.

v0:
```python
import math

import jax
import jax.numpy as jnp
from jax import lax
from jax.sharding import PartitionSpec as P

GROUP_WIDTH = 64
FACTOR = 256


highest = lax.Precision.HIGHEST


def dft_tables(count, scaling):
    first_index = lax.broadcasted_iota(jnp.int32, (count, count), 0)
    second_index = lax.broadcasted_iota(jnp.int32, (count, count), 1)
    angles = 2.0 * math.pi / count * (first_index * second_index % count).astype(jnp.float32)
    return (jnp.cos(angles) * scaling, jnp.sin(angles) * scaling)


def position_transform(real_part, imag_part, length, factor):
    columns = real_part.shape[0]
    remain = length // factor
    real_grid = real_part.reshape(columns, factor, remain)
    imag_grid = imag_part.reshape(columns, factor, remain)
    outer_cos, outer_sin = dft_tables(factor, 1.0)
    real_one = jnp.einsum("kn,cnm->ckm", outer_cos, real_grid, precision=highest) + jnp.einsum(
        "kn,cnm->ckm", outer_sin, imag_grid, precision=highest
    )
    imag_one = jnp.einsum("kn,cnm->ckm", outer_cos, imag_grid, precision=highest) - jnp.einsum(
        "kn,cnm->ckm", outer_sin, real_grid, precision=highest
    )
    outer_index = lax.broadcasted_iota(jnp.int32, (factor, remain), 0)
    inner_index = lax.broadcasted_iota(jnp.int32, (factor, remain), 1)
    angles = 2.0 * math.pi / length * (outer_index * inner_index).astype(jnp.float32)
    twist_cos = jnp.cos(angles)
    twist_sin = jnp.sin(angles)
    real_two = real_one * twist_cos + imag_one * twist_sin
    imag_two = imag_one * twist_cos - real_one * twist_sin
    inner_cos, inner_sin = dft_tables(remain, 1.0 / math.sqrt(length))
    real_out = jnp.einsum("ckn,nq->cqk", real_two, inner_cos, precision=highest) + jnp.einsum(
        "ckn,nq->cqk", imag_two, inner_sin, precision=highest
    )
    real_out = real_out.reshape(columns, length)
    return (real_out, real_out)


def local(tokens, norm_gain, in_weight, out_weight):
    rows_here = tokens.shape[0]
    channels = in_weight.shape[1]
    groups = channels // GROUP_WIDTH
    devices = lax.axis_size(("row", "col"))
    length = rows_here * devices
    floats = tokens.astype(jnp.float32)
    scaling = lax.rsqrt(jnp.mean(floats * floats, axis=-1, keepdims=True) + 1e-06)
    normed = (floats * scaling * norm_gain.astype(jnp.float32)).astype(jnp.bfloat16)
    hidden = lax.dot_general(
        in_weight, normed, (((0,), (1,)), ((), ())), preferred_element_type=jnp.float32
    ).astype(jnp.bfloat16)
    widened = (
        lax.optimization_barrier(hidden).astype(jnp.float32).reshape(groups, GROUP_WIDTH, rows_here)
    )
    channel_scale = 1.0 / math.sqrt(GROUP_WIDTH)
    chan_cos, chan_sin = dft_tables(GROUP_WIDTH, channel_scale)
    real_chan = jnp.einsum("mc,gct->gmt", chan_cos, widened, precision=highest).reshape(
        channels, rows_here
    )
    imag_chan = -jnp.einsum("mc,gct->gmt", chan_sin, widened, precision=highest).reshape(
        channels, rows_here
    )
    real_cols, imag_cols = (
        lax.all_to_all(
            real_chan.astype(jnp.bfloat16), ("row", "col"), split_axis=0, concat_axis=1, tiled=True
        ),
        lax.all_to_all(
            imag_chan.astype(jnp.bfloat16), ("row", "col"), split_axis=0, concat_axis=1, tiled=True
        ),
    )
    real_out, unused_imag = position_transform(
        real_cols.astype(jnp.float32), imag_cols.astype(jnp.float32), length, FACTOR
    )
    outgoing = real_out.astype(jnp.bfloat16)
    returned = lax.all_to_all(outgoing, ("row", "col"), split_axis=1, concat_axis=0, tiled=True)
    mixed = lax.dot_general(
        returned, out_weight, (((0,), (0,)), ((), ())), preferred_element_type=jnp.float32
    )
    return mixed.astype(jnp.bfloat16)


def solution(mesh):
    placed = (P(("row", "col"), None), P(), P(), P())
    return jax.shard_map(
        local, mesh=mesh, in_specs=placed, out_specs=P(("row", "col"), None), check_vma=False
    )
```

profile of v0, /device:TPU:1, one launch (start us, length us, event | category | flops | bytes accessed | tf_op | source)
XLA Modules:
  0.0 117.8 jit_solution(9979788294685308522)
XLA Ops:
  0.0 0.0 copy-start
  0.0 3.2 %fusion = f32[512]{0:T(512)S(1)} fusion(bf16[512,4096]{1,0:T(8,128)(2,1)} %param.4), kind=kLoop, calls=%fused_computation.2 | loop fusion | flops 6290944 | bytes 4196352 | tf_op jit(solution)/shard_map/reduce_sum | solution.py:56
  3.2 0.7 convert_element_type.88
  3.9 0.0 copy-done
  4.0 7.2 %fusion.18 = bf16[1024,512]{0,1:T(8,128)(2,1)S(1)} fusion(bf16[4096,1024]{1,0:T(8,128)(2,1)} %param.6, bf16[512,4096]{1,0:T(8,128)(2,1)S(1)} %copy-done, f32[4096]{0:T(1024)S(1)} %convert_element_type.88, f32[512]{0:T(512)S(1)} %add_rsqrt_fusion), kind=kOutput, calls=%fused_computation.23 | convolution fusion | flops 4303880192 | bytes 13649920 | tf_op jit(solution)/shard_map/dot_general | solution.py:58
  11.1 0.5 copy.27
  11.7 2.1 %negate_convert_fusion = bf16[16,512,64]{1,2,0:T(8,128)(2,1)} fusion(bf16[16,64,512]{2,1,0:T(8,128)(2,1)S(1)} %bitcast.76), kind=kOutput, calls=%fused_computation.18 | convolution fusion | flops 403763200 | bytes 2097152 | tf_op jit(solution)/shard_map/mc,gct->gmt/dot_general | solution.py:69
  13.8 11.5 %all-to-all-start.1 = ((bf16[128,8,512]{2,1,0:T(8,128)(2,1)}), bf16[128,8,512]{2,1,0:T(8,128)(2,1)S(1)}, u32[]{:S(2)}, u32[]{:S(2)}) async-start(bf16[128,8,512]{2,1,0:T(8,128)(2,1)} %bitcast.10), calls=%async_computation.1 | async-start | bytes 2097152 | tf_op jit(solution)/shard_map/all_to_all | solution.py:76
  25.3 2.1 %convolution_convert_fusion.1 = bf16[16,512,64]{1,2,0:T(8,128)(2,1)} fusion(bf16[16,64,512]{2,1,0:T(8,128)(2,1)S(1)} %bitcast.77), kind=kOutput, calls=%fused_computation.22 | convolution fusion | flops 403238912 | bytes 2097152 | tf_op jit(solution)/shard_map/mc,gct->gmt/dot_general | solution.py:66
  27.4 16.7 %all-to-all-done.1 = bf16[128,8,512]{2,1,0:T(8,128)(2,1)S(1)} async-done(((bf16[128,8,512]{2,1,0:T(8,128)(2,1)}), bf16[128,8,512]{2,1,0:T(8,128)(2,1)S(1)}, u32[]{:S(2)}, u32[]{:S(2)}) %all-to-all-start.1) | async-done | bytes 1048608 | tf_op jit(solution)/shard_map/all_to_all | solution.py:76
  44.1 4.8 %all-to-all-start = ((bf16[128,8,512]{2,1,0:T(8,128)(2,1)}), bf16[128,8,512]{2,1,0:T(8,128)(2,1)S(1)}, u32[]{:S(2)}, u32[]{:S(2)}) async-start(bf16[128,8,512]{2,1,0:T(8,128)(2,1)} %bitcast.5), calls=%async_computation | async-start | bytes 2097152 | tf_op jit(solution)/shard_map/all_to_all | solution.py:73
  48.9 1.6 %fusion.42 = (f32[256,256]{0,1:T(8,128)S(1)}, f32[256,256]{0,1:T(8,128)}) fusion(), kind=kLoop, calls=%fused_computation.48 | loop fusion | flops 196608 | bytes 524288 | tf_op jit(solution)/shard_map/sin | solution.py:38
  50.5 0.3 copy.31
  50.8 0.4 reshape.56
  51.2 16.6 %all-to-all-done = bf16[128,8,512]{2,1,0:T(8,128)(2,1)S(1)} async-done(((bf16[128,8,512]{2,1,0:T(8,128)(2,1)}), bf16[128,8,512]{2,1,0:T(8,128)(2,1)S(1)}, u32[]{:S(2)}, u32[]{:S(2)}) %all-to-all-start) | async-done | bytes 1048608 | tf_op jit(solution)/shard_map/all_to_all | solution.py:73
  67.8 0.3 copy.28
  68.1 0.6 reshape.55
  68.7 2.2 %fusion.37 = f32[8,256,256]{2,1,0:T(8,128)S(1)} fusion(bf16[8,256,256]{2,1,0:T(8,128)(2,1)S(1)} %reshape.55), kind=kOutput, calls=%fused_computation.41 | convolution fusion | flops 1611530240 | bytes 3145728 | tf_op jit(solution)/shard_map/kn,cnm->ckm/dot_general | solution.py:28
  70.8 2.2 %fusion.35 = f32[8,256,256]{2,1,0:T(8,128)S(1)} fusion(bf16[8,256,256]{2,1,0:T(8,128)(2,1)S(1)} %reshape.56), kind=kOutput, calls=%fused_computation.39 | convolution fusion | flops 1611530240 | bytes 3145728 | tf_op jit(solution)/shard_map/kn,cnm->ckm/dot_general | solution.py:31
  73.0 2.3 %convolution_add_fusion = f32[8,256,256]{2,1,0:T(8,128)S(1)} fusion(f32[8,256,256]{2,1,0:T(8,128)S(1)} %fusion.37, bf16[8,256,256]{2,1,0:T(8,128)(2,1)S(1)} %reshape.56), kind=kOutput, calls=%fused_computation.20 | convolution fusion | flops 1612054528 | bytes 5242880 | tf_op jit(solution)/shard_map/kn,cnm->ckm/dot_general | solution.py:28
  75.3 0.0 copy-start.1
  75.3 2.3 %convolution_subtract_fusion = f32[8,256,256]{2,1,0:T(8,128)S(1)} fusion(f32[8,256,256]{2,1,0:T(8,128)S(1)} %fusion.35, bf16[8,256,256]{2,1,0:T(8,128)(2,1)S(1)} %reshape.55), kind=kOutput, calls=%fused_computation.19 | convolution fusion | flops 1612054528 | bytes 5242880 | tf_op jit(solution)/shard_map/kn,cnm->ckm/dot_general | solution.py:31
  77.6 0.0 copy-done.1
  77.6 3.1 %fusion.8 = f32[256,8,256]{2,0,1:T(8,128)S(1)} fusion(f32[8,256,256]{2,1,0:T(8,128)S(1)} %convolution_subtract_fusion, f32[8,256,256]{2,1,0:T(8,128)S(1)} %convolution_add_fusion, f32[256,256]{0,1:T(8,128)S(1)} %get-tuple-element.5, f32[256,256]{0,1:T(8,128)S(1)} %copy-done.1), kind=kOutput, calls=%fused_computation.12 | convolution fusion | flops 1613168640 | bytes 6815744 | tf_op jit(solution)/shard_map/ckn,nq->cqk/dot_general | solution.py:42
  80.6 3.4 %fusion.21 = bf16[8,256,256]{2,1,0:T(8,128)(2,1)S(1)} fusion(f32[256,8,256]{2,0,1:T(8,128)S(1)} %fusion.8, f32[8,256,256]{2,1,0:T(8,128)S(1)} %convolution_subtract_fusion, f32[8,256,256]{2,1,0:T(8,128)S(1)} %convolution_add_fusion, f32[256,256]{0,1:T(8,128)S(1)} %get-tuple-element.5, f32[256,256]{0,1:T(8,128)S(1)} %copy-done.1), kind=kOutput, calls=%fused_computation.24 | convolution fusion | flops 1614217216 | bytes 7864320 | tf_op jit(solution)/shard_map/ckn,nq->cqk/dot_general | solution.py:42
  84.0 0.4 convert_element_type.102
  84.4 0.6 copy.40
  85.0 23.3 %all_to_all.42 = bf16[8,128,512]{2,0,1:T(8,128)(2,1)S(1)} all-to-all(bf16[8,128,512]{2,0,1:T(8,128)(2,1)S(1)} %copy.40), channel_id=1, replica_groups=mesh['row'=16,'col'=8] {'row','col'}, dimensions={1} | all-to-all | bytes 2097152 | tf_op jit(solution)/shard_map/all_to_all | solution.py:84
  108.3 9.5 %convolution_convert_fusion = bf16[512,4096]{1,0:T(8,128)(2,1)} fusion(bf16[1024,4096]{1,0:T(8,128)(2,1)} %param.7, bf16[8,128,512]{2,0,1:T(8,128)(2,1)S(1)} %all_to_all.42), kind=kOutput, calls=%fused_computation.5 | convolution fusion | flops 4297064448 | bytes 13631488 | tf_op jit(solution)/shard_map/dot_general | solution.py:85
  (1 shorter events, 0.0 us)
Async XLA Ops:
  0.0 4.0 %copy-start = (bf16[512,4096]{1,0:T(8,128)(2,1)S(1)}, bf16[512,4096]{1,0:T(8,128)(2,1)}, u32[]{:S(2)}) copy-start(bf16[512,4096]{1,0:T(8,128)(2,1)} %param.4) | copy-start | bytes 12582916
  13.8 30.3 %all-to-all-start.1 = ((bf16[128,8,512]{2,1,0:T(8,128)(2,1)}), bf16[128,8,512]{2,1,0:T(8,128)(2,1)S(1)}, u32[]{:S(2)}, u32[]{:S(2)}) async-start(bf16[128,8,512]{2,1,0:T(8,128)(2,1)} %bitcast.10), calls=%async_computation.1 | async-start | bytes 2097152 | tf_op jit(solution)/shard_map/all_to_all | solution.py:76
  44.1 23.7 %all-to-all-start = ((bf16[128,8,512]{2,1,0:T(8,128)(2,1)}), bf16[128,8,512]{2,1,0:T(8,128)(2,1)S(1)}, u32[]{:S(2)}, u32[]{:S(2)}) async-start(bf16[128,8,512]{2,1,0:T(8,128)(2,1)} %bitcast.5), calls=%async_computation | async-start | bytes 2097152 | tf_op jit(solution)/shard_map/all_to_all | solution.py:73
  75.3 2.3 %copy-start.1 = (f32[256,256]{0,1:T(8,128)S(1)}, f32[256,256]{0,1:T(8,128)}, u32[]{:S(2)}) copy-start(f32[256,256]{0,1:T(8,128)} %get-tuple-element.6) | copy-start | bytes 786436
where the time goes:
time: 118 us
  matrix products  36.1 us (31%)
  waiting for transfers between devices  33.3 us (28%)
  blocking collectives  23.3 us (20%)
  starting transfers between devices  16.3 us (14%)
  other arithmetic  5.57 us (5%)
  local copies, waits for them, and re-layouts  3.12 us (3%)
    all_to_all x1, blocking collectives, local(): lax.all_to_all(outgoing, ('row', 'col'), split_axis=1, concat_axis=0, til...  23.3 us
    all_to_all x1, waiting for transfers between devices, local(): lax.all_to_all(imag_chan.astype(jnp.bfloat16), ('row', 'col'), split_axis...  16.7 us
    all_to_all x1, waiting for transfers between devices, local(): lax.all_to_all(real_chan.astype(jnp.bfloat16), ('row', 'col'), split_axis...  16.6 us
    all_to_all x1, starting transfers between devices, local(): lax.all_to_all(imag_chan.astype(jnp.bfloat16), ('row', 'col'), split_axis...  11.5 us
    dot_general x1, matrix products, local(): lax.dot_general(returned, out_weight, (((0,), (0,)), ((), ())), preferred...  9.49 us
    dot_general x1, matrix products, local(): lax.dot_general(in_weight, normed, (((0,), (1,)), ((), ())), preferred_el...  7.17 us
    all_to_all x1, starting transfers between devices, local(): lax.all_to_all(real_chan.astype(jnp.bfloat16), ('row', 'col'), split_axis...  4.77 us
    dot_general x1, matrix products, position_transform(): jnp.einsum('ckn,nq->cqk', imag_two, inner_sin, precision=highest)  3.39 us
  transfers between devices with their start and end apart: 2, of which 2 were waited for; matrix products, arithmetic and copies ran while one was open for 4% of the time, Pallas kernels for 0%

commit v1 on v0

v1 whole, which is shorter than its diff:
```python
import functools
import math

import jax
import jax.numpy as jnp
import numpy as np
from jax import lax
from jax.experimental import pallas as pl
from jax.experimental.pallas import tpu as pltpu
from jax.sharding import PartitionSpec as P

ROWS = 512
WIDTH = 4096
PLANES = 4
PER = 32
CH = 8
MESH = pl.DeviceIdType.MESH
F32 = jnp.float32
BF16 = jnp.bfloat16


def channel_table():
    table = np.zeros((256, 256))
    c = np.arange(64)
    for g in range(4):
        for i in range(8):
            for ch in range(8):
                p = 4 * i + ch % 4
                if ch < 4:
                    row = np.cos(2 * np.pi * c * p / 64)
                elif p == 0:
                    row = np.cos(np.pi * c)
                else:
                    row = -np.sin(2 * np.pi * c * p / 64)
                table[g * 64 + i * 8 + ch, g * 64 : g * 64 + 64] = row / 8
    return table


def unpack_table():
    table = np.zeros((256, 256))
    for g in range(4):
        for i in range(8):
            for ch in range(4):
                p = 4 * i + ch
                real, imag = g * 64 + i * 8 + ch, g * 64 + i * 8 + ch + 4
                if p == 0:
                    table[real, g * 64] = 1
                    table[imag, g * 64 + 32] = 1
                else:
                    table[real, g * 64 + p] = 1
                    table[imag, g * 64 + p] = 1
                    table[real, g * 64 + 64 - p] = 1
                    table[imag, g * 64 + 64 - p] = -1
    return table


def swap_table():
    table = np.zeros((256, 256))
    for d in range(PER):
        for ch in range(CH):
            table[ch * PER + d, d * CH + ch] = 1
    return table


def tables():
    chan = channel_table()
    high = chan.astype(BF16)
    low = (chan - high.astype(np.float64)).astype(BF16)
    swap = swap_table()
    square = np.concatenate([high, low, swap.astype(BF16), swap.T.astype(BF16), unpack_table().astype(BF16)])
    d = np.arange(128)
    angle = 2 * np.pi * ((d[:, None] * d[None, :]) % 128) / 128
    outer = np.concatenate([np.cos(angle), -np.sin(angle)]).astype(BF16)
    j = np.arange(512)
    twist = 2 * np.pi * (d[:, None] * j[None, :]) / 65536
    twist = np.stack([np.cos(twist), np.sin(twist)]).astype(np.float32)
    e = np.arange(128).reshape(4, 1, 32)
    s = np.arange(4).reshape(1, 4, 1)
    p = (4 * e + s).reshape(512)
    angle = 2 * np.pi * ((p[:, None] * j[None, :]) % 512) / 512
    inner = (np.concatenate([np.cos(angle), np.sin(angle)], axis=1) / 256).astype(BF16)
    return square.reshape(5, 256, 256), outer, twist, inner


def coords(device):
    return {"row": device // 8, "col": device % 8}


def mixer(
    tok_hbm, gain_ref, win_hbm, square_hbm, outer_hbm, twist_hbm, inner_hbm, spec_ref,
    tok, win, square, outer, twist, inner, send1, recv1, send2, recv2, xb, ts,
    tok_sem, win_sem, tab_sem, ssem1, rsem1, ssem2, rsem2,
):
    me = lax.axis_index("row") * 8 + lax.axis_index("col")
    plane = me // PER
    place = me % PER

    barrier = pltpu.get_barrier_semaphore()

    @pl.loop(1, 128)
    def _(r):
        pl.semaphore_signal(barrier, 1, device_id=coords((me + r) % 128), device_id_type=MESH)

    tok_copies = []
    for i in range(8):
        rows = pl.ds(i * 64, 64)
        copy = pltpu.make_async_copy(tok_hbm.at[rows], tok.at[rows], tok_sem.at[i])
        copy.start()
        tok_copies.append(copy)
    win_copies = []
    for tt in range(PLANES):
        target = (plane + 1 + tt) % PLANES
        copy = pltpu.make_async_copy(
            win_hbm.at[:, pl.ds(pl.multiple_of(target * 256, 256), 256)], win.at[tt], win_sem.at[tt]
        )
        copy.start()
        win_copies.append(copy)
    tab_copies = []
    for i, (a, b) in enumerate(
        ((square_hbm, square), (outer_hbm, outer), (twist_hbm, twist), (inner_hbm, inner))
    ):
        copy = pltpu.make_async_copy(a, b, tab_sem.at[i])
        copy.start()
        tab_copies.append(copy)

    gain = gain_ref[...].astype(F32)
    for i in range(8):
        tok_copies[i].wait()

        @pl.loop(0, 4)
        def _(k):
            rows = pl.ds(pl.multiple_of(i * 64 + k * 16, 16), 16)
            x = tok[rows, :].astype(F32)
            scale = lax.rsqrt(jnp.mean(x * x, axis=-1, keepdims=True) + 1e-06)
            tok[rows, :] = (x * scale * gain).astype(BF16)

    tab_copies[0].wait()
    pl.semaphore_wait(barrier, 127)

    for tt in range(PLANES):
        target = (plane + 1 + tt) % PLANES
        win_copies[tt].wait()
        h = jnp.dot(tok[...], win[tt], preferred_element_type=F32).astype(BF16)
        dims = (((1,), (1,)), ((), ()))
        s = lax.dot_general(square[0], h, dims, preferred_element_type=F32) + lax.dot_general(
            square[1], h, dims, preferred_element_type=F32
        )
        send1[pl.ds(target * PER, PER)] = s.reshape(PER, CH, ROWS).astype(BF16)
        if tt == PLANES - 1:
            recv1[me] = send1[me]

        @pl.loop(1 if tt == PLANES - 1 else 0, PER)
        def _(r):
            dest = target * PER + (place + r) % PER
            pltpu.make_async_remote_copy(
                send1.at[dest], recv1.at[me], ssem1, rsem1.at[plane], device_id=coords(dest), device_id_type=MESH
            ).start()

    for copy in tab_copies[1:]:
        copy.wait()

    def wait_block(send, recv, sem, source, count):
        pltpu.make_async_remote_copy(
            send.at[pl.ds(0, count)], recv.at[pl.ds(0, count)], sem, sem, device_id=coords(me), device_id_type=MESH
        ).wait_recv()

    for tt in range(PLANES):
        source = (plane + 3 - tt) % PLANES
        wait_block(send1, recv1, rsem1.at[source], source, PER - (tt == PLANES - 1))
        block = recv1[pl.ds(source * PER, PER)].reshape(PER * CH, ROWS)
        x = jnp.dot(square[2], block, preferred_element_type=F32).astype(BF16)
        for ch in range(CH):
            xb[ch, pl.ds(pl.multiple_of(source * PER, PER), PER), :] = x[ch * PER : ch * PER + PER]

    special = place % 8 == 0
    for cp in range(4):
        parts = []
        for ch in (2 * cp, 2 * cp + 1):
            a = jnp.dot(outer[...], xb[ch], preferred_element_type=F32)
            re, im = a[:128], a[128:]
            b_re = re * twist[0] + im * twist[1]
            b_im = im * twist[0] - re * twist[1]
            if ch == 4:
                b_re, b_im = jnp.where(special, b_re, -b_im), jnp.where(special, b_im, b_re)
            elif ch > 4:
                b_re, b_im = -b_im, b_re
            parts.append(jnp.concatenate([b_re.astype(BF16), b_im.astype(BF16)], axis=1))
        b = jnp.concatenate(parts, axis=0)
        t = lax.dot_general(inner[...], b, (((1,), (1,)), ((), ())), preferred_element_type=F32)
        for eb in range(4):
            for s in range(4):
                for c in range(2):
                    ch = 2 * cp + c
                    ts[eb, ch * PER : ch * PER + PER, s * 128 : s * 128 + 128] = t[
                        (eb * 4 + s) * PER : (eb * 4 + s + 1) * PER, c * 128 : c * 128 + 128
                    ].astype(BF16)

    for tt in range(PLANES):
        target = (plane + 1 + tt) % PLANES
        y = jnp.dot(square[3], ts[target], preferred_element_type=F32)
        send2[pl.ds(target * PER, PER)] = y.reshape(PER, CH, ROWS).astype(BF16)
        if tt == PLANES - 1:
            recv2[me] = send2[me]

        @pl.loop(1 if tt == PLANES - 1 else 0, PER)
        def _(r):
            dest = target * PER + (place + r) % PER
            pltpu.make_async_remote_copy(
                send2.at[dest], recv2.at[me], ssem2, rsem2.at[plane], device_id=coords(dest), device_id_type=MESH
            ).start()

    for tt in range(PLANES):
        source = (plane + 3 - tt) % PLANES
        wait_block(send2, recv2, rsem2.at[source], source, PER - (tt == PLANES - 1))
        block = recv2[pl.ds(source * PER, PER)].reshape(PER * CH, ROWS)
        y = lax.dot_general(block, square[4], (((0,), (0,)), ((), ())), preferred_element_type=F32)
        spec_ref[:, pl.ds(pl.multiple_of(source * 256, 256), 256)] = y.astype(BF16)

    for send, sem in ((send1, ssem1), (send2, ssem2)):
        pltpu.make_async_remote_copy(
            send.at[pl.ds(0, 127)], send.at[pl.ds(0, 127)], sem, sem, device_id=coords(me), device_id_type=MESH
        ).wait_send()


def local(tokens, norm_gain, in_weight, out_weight):
    square, outer, twist, inner = tables()
    hbm = pl.BlockSpec(memory_space=pl.ANY)
    vmem = pl.BlockSpec(memory_space=pltpu.VMEM)
    block = pltpu.VMEM((128, CH, ROWS), BF16)
    spec = pl.pallas_call(
        mixer,
        out_shape=jax.ShapeDtypeStruct((ROWS, 1024), BF16),
        in_specs=[hbm, vmem, hbm, hbm, hbm, hbm, hbm],
        out_specs=vmem,
        scratch_shapes=[
            pltpu.VMEM((ROWS, WIDTH), BF16),
            pltpu.VMEM((PLANES, WIDTH, 256), BF16),
            pltpu.VMEM((5, 256, 256), BF16),
            pltpu.VMEM((256, 128), BF16),
            pltpu.VMEM((2, 128, 512), F32),
            pltpu.VMEM((512, 1024), BF16),
            block, block, block, block,
            pltpu.VMEM((CH, 128, 512), BF16),
            pltpu.VMEM((4, 256, 512), BF16),
            pltpu.SemaphoreType.DMA((8,)),
            pltpu.SemaphoreType.DMA((4,)),
            pltpu.SemaphoreType.DMA((4,)),
            pltpu.SemaphoreType.DMA,
            pltpu.SemaphoreType.DMA((4,)),
            pltpu.SemaphoreType.DMA,
            pltpu.SemaphoreType.DMA((4,)),
        ],
        compiler_params=pltpu.CompilerParams(
            collective_id=0, has_side_effects=True, vmem_limit_bytes=50 * 2**20
        ),
        name="mixer",
    )(tokens, norm_gain.reshape(1, WIDTH), in_weight, jnp.asarray(square), jnp.asarray(outer), jnp.asarray(twist), jnp.asarray(inner))
    mixed = jnp.dot(spec, out_weight, preferred_element_type=F32)
    return mixed.astype(BF16)


def solution(mesh):
    placed = (P(("row", "col"), None), P(), P(), P())
    return jax.shard_map(
        local, mesh=mesh, in_specs=placed, out_specs=P(("row", "col"), None), check_vma=False
    )
```

time: 118 us -> 66.1 us (0.56)
  Pallas kernels: 0 us -> 54.8 us
  waiting for transfers between devices: 33.3 us -> 0 us
  matrix products: 36.1 us -> 6.03 us
  blocking collectives: 23.3 us -> 0 us
  starting transfers between devices: 16.3 us -> 0 us
  other arithmetic: 5.57 us -> 0 us
  local copies, waits for them, and re-layouts: 3.12 us -> 4.9 us
    pallas_call x0 -> x1, Pallas kernels: none -> 54.8 us  [local(): pl.pallas_call(mixer, out_shape=jax.ShapeDtypeStruct((ROWS, 1024), BF16),...]
    all_to_all x2 -> x0, waiting for transfers between devices: 33.3 us -> none  [the longest x1 16.7 us: local(): lax.all_to_all(imag_chan.astype(jnp.bfloat16), ('row', 'col'), split_axis...]
    dot_general x10 -> x1, matrix products: 36.1 us -> 6.03 us  [local(): mixed = jnp.dot(spec, out_weight, preferred_element_type=F32)]
    all_to_all x1 -> x0, blocking collectives: 23.3 us -> none  [local(): lax.all_to_all(outgoing, ('row', 'col'), split_axis=1, concat_axis=0, til...]
    all_to_all x2 -> x0, starting transfers between devices: 16.3 us -> none  [the longest x1 11.5 us: local(): lax.all_to_all(imag_chan.astype(jnp.bfloat16), ('row', 'col'), split_axis...]
    unnamed x4 -> x10, local copies, waits for them, and re-layouts: 0.01 us -> 4.19 us
    reduce_sum x1 -> x0, other arithmetic: 3.23 us -> none  [local(): jnp.mean(floats * floats, axis=-1, keepdims=True) + 1e-06]
    sin x1 -> x0, other arithmetic: 1.63 us -> none  [position_transform(): twist_sin = jnp.sin(angles)]
  transfers between devices with their start and end apart: 2 -> 0, of which waited for: 2 -> 0; matrix products, arithmetic and copies ran while one was open for 4% -> 0% of each run, Pallas kernels for 0% -> 0%
where the time goes in v1:
time: 66.1 us; the launch traced here: 65.8 us
  Pallas kernels  54.8 us (83%)
  matrix products  6.03 us (9%)
  local copies, waits for them, and re-layouts  4.9 us (7%)
    pallas_call x1, Pallas kernels, local(): pl.pallas_call(mixer, out_shape=jax.ShapeDtypeStruct((ROWS, 1024), BF16),...  54.8 us
    dot_general x1, matrix products, local(): mixed = jnp.dot(spec, out_weight, preferred_element_type=F32)  6.03 us
    unnamed x10, local copies, waits for them, and re-layouts  4.19 us

profile of v1, /device:TPU:1, one launch (start us, length us, event | category | flops | bytes accessed | tf_op | source)
XLA Modules:
  0.0 65.8 jit_solution(7150954744224749163)
XLA Ops:
  0.0 0.7 %reshape.3.gain_ref = bf16[1,4096]{1,0:T(2,128)(2,1)S(1)} reshape(bf16[4096]{0:T(1024)(128)(2,1)} %param.9) | data formatting | bytes 16384 | tf_op jit(solution)/shard_map/reshape | solution.py:257
  0.7 0.0 copy-start
  0.7 1.2 %copy-done = bf16[512,1024]{1,0:T(8,128)(2,1)S(1)} copy-done((bf16[512,1024]{1,0:T(8,128)(2,1)S(1)}, bf16[512,1024]{1,0:T(8,128)(2,1)}, u32[]{:S(2)}) %copy-start) | copy-done | bytes 1048600
  1.9 0.0 copy-start.1
  1.9 1.1 %copy-done.1 = bf16[5,256,256]{2,1,0:T(8,128)(2,1)S(1)} copy-done((bf16[5,256,256]{2,1,0:T(8,128)(2,1)S(1)}, bf16[5,256,256]{2,1,0:T(8,128)(2,1)}, u32[]{:S(2)}) %copy-start.1) | copy-done | bytes 655384
  3.0 0.0 copy-start.2
  3.0 1.0 %copy-done.2 = f32[2,128,512]{2,1,0:T(8,128)S(1)} copy-done((f32[2,128,512]{2,1,0:T(8,128)S(1)}, f32[2,128,512]{2,1,0:T(8,128)}, u32[]{:S(2)}) %copy-start.2) | copy-done | bytes 524312
  4.1 0.0 copy-start.3
  4.1 0.8 %copy-done.3 = bf16[256,128]{1,0:T(8,128)(2,1)S(1)} copy-done((bf16[256,128]{1,0:T(8,128)(2,1)S(1)}, bf16[256,128]{1,0:T(8,128)(2,1)}, u32[]{:S(2)}) %copy-start.3) | copy-done | bytes 65560
  4.9 0.0 copy-start.4
  4.9 54.8 %mixer.1 = bf16[512,1024]{1,0:T(8,128)(2,1)S(1)} custom-call(bf16[512,4096]{1,0:T(8,128)(2,1)} %tok_hbm.1, bf16[1,4096]{1,0:T(2,128)(2,1)S(1)} %reshape.3.gain_ref, bf16[4096,1024]{1,0:T(8,128)(2,1)} %win_hbm.1, bf16[5,256,256]{2,1,0:T(8,128)(2,1)S(1)} %copy-done.1, bf16[256,128]{1,0:T(8,128)(2,1)S(1)} %copy-done.3, f32[2,128,512]{2,1,0:T(8,128)S(1)} %copy-done.2, ...), custom_call_target="tpu_custom_call" | custom-call | tf_op jit(solution)/shard_map/mixer/pallas_call | solution.py:230
  59.7 0.0 copy-done.4
  59.7 6.0 %convolution_convert_fusion = bf16[512,4096]{1,0:T(8,128)(2,1)} fusion(bf16[512,1024]{1,0:T(8,128)(2,1)S(1)} %mixer.1, bf16[1024,4096]{1,0:T(8,128)(2,1)S(1)} %copy-done.4), kind=kOutput, calls=%fused_computation | convolution fusion | flops 4297064448 | bytes 13631488 | tf_op jit(solution)/shard_map/dot_general | solution.py:258
Async XLA Ops:
  0.7 1.2 %copy-start = (bf16[512,1024]{1,0:T(8,128)(2,1)S(1)}, bf16[512,1024]{1,0:T(8,128)(2,1)}, u32[]{:S(2)}) copy-start(bf16[512,1024]{1,0:T(8,128)(2,1)} %constant.11.clone.inner_hbm) | copy-start | bytes 3145732
  1.9 1.1 %copy-start.1 = (bf16[5,256,256]{2,1,0:T(8,128)(2,1)S(1)}, bf16[5,256,256]{2,1,0:T(8,128)(2,1)}, u32[]{:S(2)}) copy-start(bf16[5,256,256]{2,1,0:T(8,128)(2,1)} %constant.8.clone.square_hbm) | copy-start | bytes 1966084
  3.0 1.0 %copy-start.2 = (f32[2,128,512]{2,1,0:T(8,128)S(1)}, f32[2,128,512]{2,1,0:T(8,128)}, u32[]{:S(2)}) copy-start(f32[2,128,512]{2,1,0:T(8,128)} %constant.10.clone.twist_hbm) | copy-start | bytes 1572868
  4.1 0.8 %copy-start.3 = (bf16[256,128]{1,0:T(8,128)(2,1)S(1)}, bf16[256,128]{1,0:T(8,128)(2,1)}, u32[]{:S(2)}) copy-start(bf16[256,128]{1,0:T(8,128)(2,1)} %constant.9.clone.outer_hbm) | copy-start | bytes 196612
  4.9 54.8 %copy-start.4 = (bf16[1024,4096]{1,0:T(8,128)(2,1)S(1)}, bf16[1024,4096]{1,0:T(8,128)(2,1)}, u32[]{:S(2)}) copy-start(bf16[1024,4096]{1,0:T(8,128)(2,1)} %param.11) | copy-start | bytes 25165828

commit v2 on v0

v2 whole, which is shorter than its diff:
```python
import functools
import math

import jax
import jax.numpy as jnp
import numpy as np
from jax import lax
from jax.experimental import pallas as pl
from jax.experimental.pallas import tpu as pltpu
from jax.sharding import PartitionSpec as P

ROWS = 512
WIDTH = 4096
PLANES = 4
PER = 32
HALF = 256
MESH = pl.DeviceIdType.MESH
F32 = jnp.float32
BF16 = jnp.bfloat16
LAST = (((1,), (1,)), ((), ()))
FIRST = (((0,), (0,)), ((), ()))


def slot_pair(half, i, slot):
    return 4 * i + 2 * half + slot % 2


def channel_table():
    table = np.zeros((2, 2, 4, 8, 2, 4, 256))
    c = np.arange(64)
    for half in range(2):
        for g in range(4):
            for i in range(8):
                for slot in range(4):
                    p = slot_pair(half, i, slot)
                    if slot < 2:
                        row = np.cos(2 * np.pi * c * p / 64)
                    elif p == 0:
                        row = np.cos(np.pi * c)
                    else:
                        row = -np.sin(2 * np.pi * c * p / 64)
                    for h in range(2):
                        table[h, half, g, i, h, slot, g * 64 : g * 64 + 64] = row / 8
    return table.reshape(2, 512, 256)


def weight_table():
    table = np.zeros((2, 4, 4, 8, 4, 64))
    for half in range(2):
        for g in range(4):
            for i in range(8):
                for slot in range(4):
                    p = slot_pair(half, i, slot)
                    if p == 0:
                        table[half, slot, g, i, g, 0 if slot < 2 else 32] = 1
                    else:
                        table[half, slot, g, i, g, p] = 1
                        table[half, slot, g, i, g, 64 - p] = 1 if slot < 2 else -1
    return table.reshape(256, 256)


def swap_table():
    table = np.zeros((256, 256))
    for d in range(PER):
        for slot in range(8):
            table[slot * PER + d, d * 8 + slot] = 1
    return table


def tables():
    chan = channel_table()
    high = chan.astype(BF16)
    low = (chan - high.astype(np.float64)).astype(BF16)
    chan = np.stack([high, low])
    swap = swap_table()
    square = np.stack([swap, swap.T, weight_table()]).astype(BF16)
    d = np.arange(128)
    angle = 2 * np.pi * ((d[:, None] * d[None, :]) % 128) / 128
    outer = np.concatenate([np.cos(angle), -np.sin(angle)]).astype(BF16)
    j = np.arange(512)
    e = np.arange(128).reshape(4, 1, 32)
    s = np.arange(4).reshape(1, 4, 1)
    p = (4 * e + s).reshape(512)
    angle = 2 * np.pi * ((p[:, None] * j[None, :]) % 512) / 512
    inner = (np.concatenate([np.cos(angle), np.sin(angle)], axis=1) / 256).astype(BF16)
    return chan, square, outer, inner


def series(first, count):
    return [
        (-1) ** k * (2 * math.pi) ** (2 * k + first) / math.factorial(2 * k + first) for k in range(count)
    ]


def polynomial(t, coefficients):
    total = jnp.full_like(t, coefficients[-1])
    for c in coefficients[-2::-1]:
        total = total * t + c
    return total


STEPS = [
    (x, y, c)
    for x, y in sorted(
        ((x, y) for x in range(4) for y in range(4)), key=lambda s: -min(s[0], 4 - s[0]) - min(s[1], 4 - s[1])
    )
    for c in (1, 0)
]


def when(condition, action):
    if isinstance(condition, bool):
        if condition:
            action()
    else:
        pl.when(condition)(action)


def plane_step(tt):
    high, low = tt // 2, tt % 2
    return 2 - low + high - 2 * low * high


def mixer(
    tok_hbm, gain_hbm, win_hbm, wout_hbm, chan_hbm, square_hbm, outer_hbm, inner_hbm,
    acc, spec_b, wmix_b,
    tok, gain_ref, win, wout, wmix_a, chan, square, outer, twist, inner,
    hs, send, recv, xb, ts, spec_a,
    tok_sem, win_sem, tab_sem, ssem, rsem,
):
    row, col = lax.axis_index("row"), lax.axis_index("col")
    me = row * 8 + col
    plane, x = lax.div(row, 4), lax.rem(row, 4)
    y, core = lax.div(col, 2), lax.rem(col, 2)
    xs = [lax.rem(x + i, 4) for i in range(4)]
    cols = [[lax.rem(y + i, 4) * 2 + (core if c == 0 else 1 - core) for c in range(2)] for i in range(4)]

    gain_copy = pltpu.make_async_copy(gain_hbm, gain_ref, tab_sem.at[0])
    gain_copy.start()
    tok_copies = []
    for i in range(8):
        rows = pl.ds(i * 64, 64)
        copy = pltpu.make_async_copy(tok_hbm.at[rows], tok.at[rows], tok_sem.at[i])
        tok_copies.append(copy)

    def win_copy(tt):
        target = lax.rem(plane + plane_step(tt), 4)
        columns = pl.ds(pl.multiple_of(target * 256, 256), 256)
        return pltpu.make_async_copy(win_hbm.at[:, columns], win.at[tt], win_sem.at[tt])

    copies = {}
    for i, (name, a, b) in enumerate(
        (
            ("chan", chan_hbm, chan), ("square", square_hbm, square), ("outer", outer_hbm, outer),
            ("inner", inner_hbm, inner), ("wout", wout_hbm, wout),
        )
    ):
        copies[name] = pltpu.make_async_copy(a, b, tab_sem.at[i + 1])
    for i in range(3):
        tok_copies[i].start()
    win_copy(0).start()
    for i in range(3, 8):
        tok_copies[i].start()
    barrier = pltpu.get_barrier_semaphore()

    @pl.loop(0, 16)
    def _(d):
        to_row = lax.rem(plane + 2 + lax.div(d, 4), 4) * 4 + lax.rem(x + d, 4)
        for dy in range(4):
            for dc in range(2):
                to_col = cols[dy][dc]

                def signal():
                    pl.semaphore_signal(barrier, 1, device_id={"row": to_row, "col": to_col}, device_id_type=MESH)

                if dy == 0 and dc == 0:
                    pl.when(to_row != row)(signal)
                else:
                    signal()

    gain_copy.wait()
    gain = gain_ref[...].astype(F32).reshape(1, WIDTH)

    def first_tile(k):
        rows = slice(k * 128, k * 128 + 128)
        hs[0, rows, :] = jnp.dot(tok[rows, :], win[0], preferred_element_type=F32).astype(BF16)

    for i in range(4):
        tok_copies[2 * i].wait()
        tok_copies[2 * i + 1].wait()
        if i == 1:
            win_copy(0).wait()
        if i > 0:
            first_tile(i - 1)
        for k in range(2):
            rows = slice(i * 128 + k * 64, i * 128 + k * 64 + 64)
            v = tok[rows, :].astype(F32)
            scale = lax.rsqrt(jnp.mean(v * v, axis=-1, keepdims=True) + 1e-06)
            tok[rows, :] = (v * scale * gain).astype(BF16)
        if i == 0:
            copies["chan"].start()
            win_copy(1).start()
        if i == 1:
            win_copy(2).start()
            win_copy(3).start()
    first_tile(3)
    copies["chan"].wait()
    for name in ("wout", "square", "outer", "inner"):
        copies[name].start()

    def exchange(stage, half, tt):
        target = lax.rem(plane + plane_step(tt), 4)
        src, dst = send.at[stage, half], recv.at[stage, half]
        for step in STEPS:
            dx, dy, dc = step
            to_row, to_col = target * 4 + xs[dx], cols[dy][dc]

            def start():
                pltpu.make_async_remote_copy(
                    src.at[to_row * 8 + to_col], dst.at[me], ssem.at[stage, half], rsem.at[stage, half, plane],
                    device_id={"row": to_row, "col": to_col}, device_id_type=MESH,
                ).start()

            if step == (0, 0, 0):
                when(tt != PLANES - 1, start)
            else:
                start()

        def keep():
            recv[stage, half, me] = send[stage, half, me]

        when(tt == PLANES - 1, keep)

    def arrive(stage, half, tt):
        source = lax.rem(plane + 4 - plane_step(tt), 4)

        def wait(count):
            ref = recv.at[stage, half, pl.ds(0, count)]
            pltpu.make_async_remote_copy(
                ref, ref, ssem.at[stage, half], rsem.at[stage, half, source],
                device_id={"row": row, "col": col}, device_id_type=MESH,
            ).wait_recv()

        when(tt != PLANES - 1, lambda: wait(PER))
        when(tt == PLANES - 1, lambda: wait(PER - 1))
        return source

    def block_of(stage, half, source):
        return recv[stage, half, pl.ds(source * PER, PER)].reshape(256, HALF)

    def channels(half, tt):
        target = lax.rem(plane + plane_step(tt), 4)
        rows = pl.ds(half * 256, 256)
        v = sum(
            lax.dot_general(
                chan[part, j, rows], hs[tt, j * HALF : j * HALF + HALF], LAST, preferred_element_type=F32
            )
            for j in range(2)
            for part in range(2)
        )
        send[0, half, pl.ds(target * PER, PER)] = v.reshape(PER, 8, HALF).astype(BF16)

    channels(0, 0)
    pl.semaphore_wait(barrier, 127)
    exchange(0, 0, 0)

    @pl.loop(1, PLANES)
    def _(tt):
        win_copy(tt).wait()
        hs[tt] = jnp.dot(tok[...], win[tt], preferred_element_type=F32).astype(BF16)
        channels(0, tt)
        exchange(0, 0, tt)

    @pl.loop(0, PLANES)
    def _(tt):
        channels(1, tt)
        exchange(0, 1, tt)

    @pl.loop(0, 8)
    def _(i):
        rows = pl.ds(pl.multiple_of(i * 16, 16), 16)
        q = lax.broadcasted_iota(jnp.int32, (16, ROWS), 0) + i * 16
        j = lax.broadcasted_iota(jnp.int32, (16, ROWS), 1)
        turns = (q * j).astype(F32) * (1.0 / 65536) - 0.5
        square_turns = turns * turns
        twist[0, rows, :] = -polynomial(square_turns, series(0, 11))
        twist[1, rows, :] = -polynomial(square_turns, series(1, 11)) * turns

    for name in ("square", "outer", "inner"):
        copies[name].wait()

    special = lax.rem(me, 8) == 0
    for half in range(2):

        @pl.loop(0, PLANES)
        def _(tt):
            source = arrive(0, half, tt)
            v = jnp.dot(square[0], block_of(0, half, source), preferred_element_type=F32).astype(BF16)
            for h in range(2):
                for slot in range(4):
                    xb[slot, pl.ds(pl.multiple_of(source * PER, PER), PER), h * HALF : h * HALF + HALF] = v[
                        (h * 4 + slot) * PER : (h * 4 + slot + 1) * PER
                    ]

        for cp in range(2):
            parts = []
            for slot in (2 * cp, 2 * cp + 1):
                a = jnp.dot(outer[...], xb[slot], preferred_element_type=F32)
                re, im = a[:128], a[128:]
                b_re = re * twist[0] + im * twist[1]
                b_im = im * twist[0] - re * twist[1]
                if half == 0 and slot == 2:
                    b_re, b_im = jnp.where(special, b_re, -b_im), jnp.where(special, b_im, b_re)
                elif slot >= 2:
                    b_re, b_im = -b_im, b_re
                parts.append(jnp.concatenate([b_re.astype(BF16), b_im.astype(BF16)], axis=1))
            b = jnp.concatenate(parts, axis=0)
            t = lax.dot_general(inner[...], b, LAST, preferred_element_type=F32)
            for eb in range(4):
                for s in range(4):
                    for c in range(2):
                        place = (s // 2) * 4 + 2 * cp + c
                        ts[eb, place * PER : place * PER + PER, s % 2 * 128 : s % 2 * 128 + 128] = t[
                            (eb * 4 + s) * PER : (eb * 4 + s + 1) * PER, c * 128 : c * 128 + 128
                        ].astype(BF16)

        @pl.loop(0, PLANES)
        def _(tt):
            target = lax.rem(plane + plane_step(tt), 4)
            v = jnp.dot(square[1], ts[target], preferred_element_type=F32)
            send[1, half, pl.ds(target * PER, PER)] = v.reshape(PER, 8, HALF).astype(BF16)
            exchange(1, half, tt)

    copies["wout"].wait()

    @pl.loop(0, PLANES)
    def _(z):
        rows = pl.ds(pl.multiple_of(z * 256, 256), 256)
        half_rows = pl.ds(pl.multiple_of(z * 128, 128), 128)

        @pl.loop(0, 1)
        def _(n):
            columns = pl.ds(pl.multiple_of(n * 4096, 4096), 4096)
            w = jnp.dot(square[2], wout[rows, columns], preferred_element_type=F32).astype(BF16)
            wmix_a[half_rows, columns] = w[:128]
            wmix_b[half_rows, columns] = w[128:]

    for half, spec in enumerate((spec_a, spec_b)):
        for tt in range(PLANES):
            arrive(1, half, tt)
        for z in range(PLANES):
            v = lax.dot_general(block_of(1, half, z), square[1], FIRST, preferred_element_type=F32).astype(BF16)
            spec[:HALF, z * 128 : z * 128 + 128] = v[:, :128]
            spec[HALF:, z * 128 : z * 128 + 128] = v[:, 128:]

        if half == 0:
            @pl.loop(0, 4)
            def _(n):
                columns = pl.ds(pl.multiple_of(n * 1024, 1024), 1024)
                acc[:, columns] = jnp.dot(spec_a[...], wmix_a[:, columns], preferred_element_type=F32)

    for stage in range(2):
        for half in range(2):
            ref = send.at[stage, half, pl.ds(0, 127)]
            pltpu.make_async_remote_copy(
                ref, ref, ssem.at[stage, half], rsem.at[stage, half, 0],
                device_id={"row": row, "col": col}, device_id_type=MESH,
            ).wait_send()


def finish(acc, spec_b, wmix_b, out_hbm, buf, sem):
    copies = []
    for n in range(8):
        columns = pl.ds(n * 512, 512)
        v = jnp.dot(spec_b[...], wmix_b[:, columns], preferred_element_type=F32)
        buf[n] = (acc[:, columns] + v).astype(BF16)
        copies.append(pltpu.make_async_copy(buf.at[n], out_hbm.at[:, columns], sem.at[n]))
        copies[n].start()
    for copy in copies:
        copy.wait()


def local(tokens, norm_gain, in_weight, out_weight):
    constants = [pltpu.with_memory_space_constraint(jnp.asarray(t), pltpu.HBM) for t in tables()]
    tokens, norm_gain, in_weight, out_weight = (
        pltpu.with_memory_space_constraint(a, pltpu.HBM) for a in (tokens, norm_gain, in_weight, out_weight)
    )
    hbm = pl.BlockSpec(memory_space=pltpu.HBM)
    vmem = pl.BlockSpec(memory_space=pltpu.VMEM)
    acc, spec_b, wmix_b = pl.pallas_call(
        mixer,
        out_shape=[
            jax.ShapeDtypeStruct((ROWS, WIDTH), F32),
            jax.ShapeDtypeStruct((ROWS, 512), BF16),
            jax.ShapeDtypeStruct((512, WIDTH), BF16),
        ],
        in_specs=[hbm] * 8,
        out_specs=[vmem] * 3,
        scratch_shapes=[
            pltpu.VMEM((ROWS, WIDTH), BF16),
            pltpu.VMEM((WIDTH,), BF16),
            pltpu.VMEM((PLANES, WIDTH, 256), BF16),
            pltpu.VMEM((1024, WIDTH), BF16),
            pltpu.VMEM((512, WIDTH), BF16),
            pltpu.VMEM((2, 2, 512, 256), BF16),
            pltpu.VMEM((3, 256, 256), BF16),
            pltpu.VMEM((256, 128), BF16),
            pltpu.VMEM((2, 128, 512), F32),
            pltpu.VMEM((512, 1024), BF16),
            pltpu.VMEM((PLANES, ROWS, 256), BF16),
            pltpu.VMEM((2, 2, 128, 8, HALF), BF16),
            pltpu.VMEM((2, 2, 128, 8, HALF), BF16),
            pltpu.VMEM((4, 128, 512), BF16),
            pltpu.VMEM((4, 256, HALF), BF16),
            pltpu.VMEM((ROWS, 512), BF16),
            pltpu.SemaphoreType.DMA((8,)),
            pltpu.SemaphoreType.DMA((4,)),
            pltpu.SemaphoreType.DMA((7,)),
            pltpu.SemaphoreType.DMA((2, 2)),
            pltpu.SemaphoreType.DMA((2, 2, 4)),
        ],
        compiler_params=pltpu.CompilerParams(
            collective_id=0, has_side_effects=True, vmem_limit_bytes=MIXER_VMEM
        ),
        name="mixer",
    )(tokens, norm_gain, in_weight, out_weight, *constants)
    return pl.pallas_call(
        finish,
        out_shape=jax.ShapeDtypeStruct((ROWS, WIDTH), BF16),
        in_specs=[vmem] * 3,
        out_specs=hbm,
        scratch_shapes=[pltpu.VMEM((8, ROWS, 512), BF16), pltpu.SemaphoreType.DMA((8,))],
        compiler_params=pltpu.CompilerParams(vmem_limit_bytes=FINISH_VMEM),
        name="finish",
    )(acc, spec_b, wmix_b)


MIXER_VMEM = 40 * 2**20
FINISH_VMEM = 8 * 2**20


def solution(mesh):
    placed = (P(("row", "col"), None), P(), P(), P())
    return jax.shard_map(
        local, mesh=mesh, in_specs=placed, out_specs=P(("row", "col"), None), check_vma=False
    )
```

time: 118 us -> 45 us (0.38)
  the two profiles are of different devices: /device:TPU:1 before, /device:TPU:0 now
where the time goes in v2:
time: 45 us; the launch traced here: 44.9 us
  Pallas kernels  44.9 us (100%)
    pallas_call x1, Pallas kernels, local(): pl.pallas_call(mixer, out_shape=[jax.ShapeDtypeStruct((ROWS, WIDTH), F32)...  41.7 us
    pallas_call x1, Pallas kernels, local(): pl.pallas_call(finish, out_shape=jax.ShapeDtypeStruct((ROWS, WIDTH), BF16...  3.22 us

profile of v2, /device:TPU:0, one launch (start us, length us, event | category | flops | bytes accessed | tf_op | source)
XLA Modules:
  0.0 44.9 jit_solution(13723245509265430305)
XLA Ops:
  0.0 41.7 %mixer.1 = (f32[512,4096]{1,0:T(8,128)S(1)}, bf16[512,512]{1,0:T(8,128)(2,1)S(1)}, bf16[512,4096]{1,0:T(8,128)(2,1)S(1)}) custom-call(bf16[512,4096]{1,0:T(8,128)(2,1)} %tok_hbm.1, bf16[4096]{0:T(1024)(128)(2,1)} %gain_hbm.1, bf16[4096,1024]{1,0:T(8,128)(2,1)} %win_hbm.1, bf16[1024,4096]{1,0:T(8,128)(2,1)} %wout_hbm.1, ...), custom_call_target="tpu_custom_call" | custom-call | tf_op jit(solution)/shard_map/mixer/pallas_call | solution.py:390
  41.7 3.2 %finish.1 = bf16[512,4096]{1,0:T(8,128)(2,1)} custom-call(f32[512,4096]{1,0:T(8,128)S(1)} %get-tuple-element.8.acc, bf16[512,512]{1,0:T(8,128)(2,1)S(1)} %get-tuple-element.9.spec_b, bf16[512,4096]{1,0:T(8,128)(2,1)S(1)} %get-tuple-element.10.wmix_b), custom_call_target="tpu_custom_call" | custom-call | tf_op jit(solution)/shard_map/finish/pallas_call | solution.py:427

commit v3 on v2

--- a/solution.py
+++ b/solution.py
@@ -1,5 +1,5 @@
-import functools
 import math
+import random
 
 import jax
 import jax.numpy as jnp
@@ -76,7 +76,9 @@
     square = np.stack([swap, swap.T, weight_table()]).astype(BF16)
     d = np.arange(128)
     angle = 2 * np.pi * ((d[:, None] * d[None, :]) % 128) / 128
-    outer = np.concatenate([np.cos(angle), -np.sin(angle)]).astype(BF16)
+    outer = np.concatenate([np.cos(angle), -np.sin(angle)])
+    outer_high = outer.astype(BF16)
+    outer = np.concatenate([outer_high, (outer - outer_high.astype(np.float64)).astype(BF16)], axis=1)
     j = np.arange(512)
     e = np.arange(128).reshape(4, 1, 32)
     s = np.arange(4).reshape(1, 4, 1)
@@ -99,13 +101,19 @@
     return total
 
 
-STEPS = [
-    (x, y, c)
-    for x, y in sorted(
-        ((x, y) for x in range(4) for y in range(4)), key=lambda s: -min(s[0], 4 - s[0]) - min(s[1], 4 - s[1])
-    )
-    for c in (1, 0)
+def hops(*steps):
+    return sum(min(s, 4 - s) for s in steps)
+
+
+EVERY = [
+    (a, b, c, d) for a in range(4) for b in range(4) for c in range(4) for d in range(2) if (a, b, c, d) != (0, 0, 0, 0)
 ]
+random.Random(2).shuffle(EVERY)
+EVERY.sort(key=lambda s: -hops(*s[:3]))
+STEPS = [(b, c, d) for b in range(4) for c in range(4) for d in range(2) if (b, c, d) != (0, 0, 0)]
+random.Random(3).shuffle(STEPS)
+STEPS.sort(key=lambda s: -hops(*s[:2]))
+STEPS.append((0, 0, 0))
 
 
 def when(condition, action):
@@ -132,6 +140,7 @@
     me = row * 8 + col
     plane, x = lax.div(row, 4), lax.rem(row, 4)
     y, core = lax.div(col, 2), lax.rem(col, 2)
+    planes = [lax.rem(plane + i, 4) for i in range(4)]
     xs = [lax.rem(x + i, 4) for i in range(4)]
     cols = [[lax.rem(y + i, 4) * 2 + (core if c == 0 else 1 - core) for c in range(2)] for i in range(4)]
 
@@ -181,29 +190,20 @@
     gain_copy.wait()
     gain = gain_ref[...].astype(F32).reshape(1, WIDTH)
 
-    def first_tile(k):
-        rows = slice(k * 128, k * 128 + 128)
-        hs[0, rows, :] = jnp.dot(tok[rows, :], win[0], preferred_element_type=F32).astype(BF16)
-
-    for i in range(4):
-        tok_copies[2 * i].wait()
-        tok_copies[2 * i + 1].wait()
+    for i in range(8):
+        tok_copies[i].wait()
+        rows = slice(i * 64, i * 64 + 64)
+        v = tok[rows, :].astype(F32)
+        scale = lax.rsqrt(jnp.mean(v * v, axis=-1, keepdims=True) + 1e-06)
+        tok[rows, :] = (v * scale * gain).astype(BF16)
         if i == 1:
-            win_copy(0).wait()
-        if i > 0:
-            first_tile(i - 1)
-        for k in range(2):
-            rows = slice(i * 128 + k * 64, i * 128 + k * 64 + 64)
-            v = tok[rows, :].astype(F32)
-            scale = lax.rsqrt(jnp.mean(v * v, axis=-1, keepdims=True) + 1e-06)
-            tok[rows, :] = (v * scale * gain).astype(BF16)
-        if i == 0:
             copies["chan"].start()
             win_copy(1).start()
-        if i == 1:
+        if i == 3:
             win_copy(2).start()
             win_copy(3).start()
-    first_tile(3)
+    win_copy(0).wait()
+    hs[0] = jnp.dot(tok[...], win[0], preferred_element_type=F32).astype(BF16)
     copies["chan"].wait()
     for name in ("wout", "square", "outer", "inner"):
         copies[name].start()
@@ -230,6 +230,16 @@
             recv[stage, half, me] = send[stage, half, me]
 
         when(tt == PLANES - 1, keep)
+
+    def exchange_all(stage, half):
+        src, dst = send.at[stage, half], recv.at[stage, half]
+        for dz, dx, dy, dc in EVERY:
+            to_row, to_col = planes[dz] * 4 + xs[dx], cols[dy][dc]
+            pltpu.make_async_remote_copy(
+                src.at[to_row * 8 + to_col], dst.at[me], ssem.at[stage, half], rsem.at[stage, half, plane],
+                device_id={"row": to_row, "col": to_col}, device_id_type=MESH,
+            ).start()
+        recv[stage, half, me] = send[stage, half, me]
 
     def arrive(stage, half, tt):
         source = lax.rem(plane + 4 - plane_step(tt), 4)
@@ -276,6 +286,7 @@
         channels(1, tt)
         exchange(0, 1, tt)
 
+
     @pl.loop(0, 8)
     def _(i):
         rows = pl.ds(pl.multiple_of(i * 16, 16), 16)
@@ -290,7 +301,9 @@
         copies[name].wait()
 
     special = lax.rem(me, 8) == 0
-    for half in range(2):
+    @pl.loop(0, 2)
+    def _(half):
+        alike = jnp.logical_and(special, half == 0)
 
         @pl.loop(0, PLANES)
         def _(tt):
@@ -305,12 +318,14 @@
         for cp in range(2):
             parts = []
             for slot in (2 * cp, 2 * cp + 1):
-                a = jnp.dot(outer[...], xb[slot], preferred_element_type=F32)
+                a = jnp.dot(
+                    outer[...], jnp.concatenate([xb[slot], xb[slot]], axis=0), preferred_element_type=F32
+                )
                 re, im = a[:128], a[128:]
                 b_re = re * twist[0] + im * twist[1]
                 b_im = im * twist[0] - re * twist[1]
-                if half == 0 and slot == 2:
-                    b_re, b_im = jnp.where(special, b_re, -b_im), jnp.where(special, b_im, b_re)
+                if slot == 2:
+                    b_re, b_im = jnp.where(alike, b_re, -b_im), jnp.where(alike, b_im, b_re)
                 elif slot >= 2:
                     b_re, b_im = -b_im, b_re
                 parts.append(jnp.concatenate([b_re.astype(BF16), b_im.astype(BF16)], axis=1))
@@ -324,11 +339,10 @@
                             (eb * 4 + s) * PER : (eb * 4 + s + 1) * PER, c * 128 : c * 128 + 128
                         ].astype(BF16)
 
-        @pl.loop(0, PLANES)
-        def _(tt):
-            target = lax.rem(plane + plane_step(tt), 4)
-            v = jnp.dot(square[1], ts[target], preferred_element_type=F32)
-            send[1, half, pl.ds(target * PER, PER)] = v.reshape(PER, 8, HALF).astype(BF16)
+        for z in range(PLANES):
+            v = jnp.dot(square[1], ts[z], preferred_element_type=F32)
+            send[1, half, z * PER : z * PER + PER] = v.reshape(PER, 8, HALF).astype(BF16)
+        for tt in range(PLANES):
             exchange(1, half, tt)
 
     copies["wout"].wait()
@@ -404,7 +418,7 @@
             pltpu.VMEM((512, WIDTH), BF16),
             pltpu.VMEM((2, 2, 512, 256), BF16),
             pltpu.VMEM((3, 256, 256), BF16),
-            pltpu.VMEM((256, 128), BF16),
+            pltpu.VMEM((256, 256), BF16),
             pltpu.VMEM((2, 128, 512), F32),
             pltpu.VMEM((512, 1024), BF16),
             pltpu.VMEM((PLANES, ROWS, 256), BF16),

time: 45 us -> 43.2 us (0.960)
  the two profiles are of different devices: /device:TPU:0 before, /device:TPU:1 now
where the time goes in v3:
time: 43.2 us; the launch traced here: 42.4 us
  Pallas kernels  42.4 us (98%)
    pallas_call x1, Pallas kernels, local(): pl.pallas_call(mixer, out_shape=[jax.ShapeDtypeStruct((ROWS, WIDTH), F32)...  39.2 us
    pallas_call x1, Pallas kernels, local(): pl.pallas_call(finish, out_shape=jax.ShapeDtypeStruct((ROWS, WIDTH), BF16...  3.22 us

profile of v3, /device:TPU:1, one launch (start us, length us, event | category | flops | bytes accessed | tf_op | source)
XLA Modules:
  0.0 42.4 jit_solution(17839240003520803696)
XLA Ops:
  0.0 39.2 %mixer.1 = (f32[512,4096]{1,0:T(8,128)S(1)}, bf16[512,512]{1,0:T(8,128)(2,1)S(1)}, bf16[512,4096]{1,0:T(8,128)(2,1)S(1)}) custom-call(bf16[512,4096]{1,0:T(8,128)(2,1)} %tok_hbm.1, bf16[4096]{0:T(1024)(128)(2,1)} %gain_hbm.1, bf16[4096,1024]{1,0:T(8,128)(2,1)} %win_hbm.1, bf16[1024,4096]{1,0:T(8,128)(2,1)} %wout_hbm.1, ...), custom_call_target="tpu_custom_call" | custom-call | tf_op jit(solution)/shard_map/mixer/pallas_call | solution.py:404
  39.2 3.2 %finish.1 = bf16[512,4096]{1,0:T(8,128)(2,1)} custom-call(f32[512,4096]{1,0:T(8,128)S(1)} %get-tuple-element.8.acc, bf16[512,512]{1,0:T(8,128)(2,1)S(1)} %get-tuple-element.9.spec_b, bf16[512,4096]{1,0:T(8,128)(2,1)S(1)} %get-tuple-element.10.wmix_b), custom_call_target="tpu_custom_call" | custom-call | tf_op jit(solution)/shard_map/finish/pallas_call | solution.py:441

commit v4 on v3

--- a/solution.py
+++ b/solution.py
@@ -125,8 +125,10 @@
 
 
 def plane_step(tt):
-    high, low = tt // 2, tt % 2
-    return 2 - low + high - 2 * low * high
+    steps = (1, 2, 3, 0)
+    if isinstance(tt, int):
+        return steps[tt]
+    return sum(jnp.where(tt == i, step, 0) for i, step in enumerate(steps))
 
 
 def mixer(
@@ -368,9 +370,9 @@
             spec[HALF:, z * 128 : z * 128 + 128] = v[:, 128:]
 
         if half == 0:
-            @pl.loop(0, 4)
+            @pl.loop(0, 2)
             def _(n):
-                columns = pl.ds(pl.multiple_of(n * 1024, 1024), 1024)
+                columns = pl.ds(pl.multiple_of(n * 2048, 2048), 2048)
                 acc[:, columns] = jnp.dot(spec_a[...], wmix_a[:, columns], preferred_element_type=F32)
 
     for stage in range(2):

time: 43.2 us -> 42.7 us (0.988); the launches traced: 42.4 us -> 42.6 us
  no operation moved by 1% of the time
where the time goes in v4:
time: 42.7 us; the launch traced here: 42.6 us
  Pallas kernels  42.6 us (100%)
    pallas_call x1, Pallas kernels, local(): pl.pallas_call(mixer, out_shape=[jax.ShapeDtypeStruct((ROWS, WIDTH), F32)...  39.4 us
    pallas_call x1, Pallas kernels, local(): pl.pallas_call(finish, out_shape=jax.ShapeDtypeStruct((ROWS, WIDTH), BF16...  3.22 us

profile of v4, /device:TPU:1, one launch (start us, length us, event | category | flops | bytes accessed | tf_op | source)
XLA Modules:
  0.0 42.6 jit_solution(7904573682997784998)
XLA Ops:
  0.0 39.4 %mixer.1 = (f32[512,4096]{1,0:T(8,128)S(1)}, bf16[512,512]{1,0:T(8,128)(2,1)S(1)}, bf16[512,4096]{1,0:T(8,128)(2,1)S(1)}) custom-call(bf16[512,4096]{1,0:T(8,128)(2,1)} %tok_hbm.1, bf16[4096]{0:T(1024)(128)(2,1)} %gain_hbm.1, bf16[4096,1024]{1,0:T(8,128)(2,1)} %win_hbm.1, bf16[1024,4096]{1,0:T(8,128)(2,1)} %wout_hbm.1, ...), custom_call_target="tpu_custom_call" | custom-call | tf_op jit(solution)/shard_map/mixer/pallas_call | solution.py:406
  39.4 3.2 %finish.1 = bf16[512,4096]{1,0:T(8,128)(2,1)} custom-call(f32[512,4096]{1,0:T(8,128)S(1)} %get-tuple-element.8.acc, bf16[512,512]{1,0:T(8,128)(2,1)S(1)} %get-tuple-element.9.spec_b, bf16[512,4096]{1,0:T(8,128)(2,1)S(1)} %get-tuple-element.10.wmix_b), custom_call_target="tpu_custom_call" | custom-call | tf_op jit(solution)/shard_map/finish/pallas_call | solution.py:443

commit v5 on v4

--- a/solution.py
+++ b/solution.py
@@ -76,9 +76,7 @@
     square = np.stack([swap, swap.T, weight_table()]).astype(BF16)
     d = np.arange(128)
     angle = 2 * np.pi * ((d[:, None] * d[None, :]) % 128) / 128
-    outer = np.concatenate([np.cos(angle), -np.sin(angle)])
-    outer_high = outer.astype(BF16)
-    outer = np.concatenate([outer_high, (outer - outer_high.astype(np.float64)).astype(BF16)], axis=1)
+    outer = np.concatenate([np.cos(angle), -np.sin(angle)]).astype(BF16)
     j = np.arange(512)
     e = np.arange(128).reshape(4, 1, 32)
     s = np.arange(4).reshape(1, 4, 1)
@@ -320,9 +318,7 @@
         for cp in range(2):
             parts = []
             for slot in (2 * cp, 2 * cp + 1):
-                a = jnp.dot(
-                    outer[...], jnp.concatenate([xb[slot], xb[slot]], axis=0), preferred_element_type=F32
-                )
+                a = jnp.dot(outer[...], xb[slot], preferred_element_type=F32)
                 re, im = a[:128], a[128:]
                 b_re = re * twist[0] + im * twist[1]
                 b_im = im * twist[0] - re * twist[1]
@@ -420,7 +416,7 @@
             pltpu.VMEM((512, WIDTH), BF16),
             pltpu.VMEM((2, 2, 512, 256), BF16),
             pltpu.VMEM((3, 256, 256), BF16),
-            pltpu.VMEM((256, 256), BF16),
+            pltpu.VMEM((256, 128), BF16),
             pltpu.VMEM((2, 128, 512), F32),
             pltpu.VMEM((512, 1024), BF16),
             pltpu.VMEM((PLANES, ROWS, 256), BF16),

time: 42.7 us -> 42.7 us (level)
  no operation moved by 1% of the time
where the time goes in v5:
time: 42.7 us; the launch traced here: 42.6 us
  Pallas kernels  42.6 us (100%)
    pallas_call x1, Pallas kernels, local(): pl.pallas_call(mixer, out_shape=[jax.ShapeDtypeStruct((ROWS, WIDTH), F32)...  39.4 us
    pallas_call x1, Pallas kernels, local(): pl.pallas_call(finish, out_shape=jax.ShapeDtypeStruct((ROWS, WIDTH), BF16...  3.22 us

profile of v5, /device:TPU:1, one launch (start us, length us, event | category | flops | bytes accessed | tf_op | source)
XLA Modules:
  0.0 42.6 jit_solution(11705417080058402516)
XLA Ops:
  0.0 39.4 %mixer.1 = (f32[512,4096]{1,0:T(8,128)S(1)}, bf16[512,512]{1,0:T(8,128)(2,1)S(1)}, bf16[512,4096]{1,0:T(8,128)(2,1)S(1)}) custom-call(bf16[512,4096]{1,0:T(8,128)(2,1)} %tok_hbm.1, bf16[4096]{0:T(1024)(128)(2,1)} %gain_hbm.1, bf16[4096,1024]{1,0:T(8,128)(2,1)} %win_hbm.1, bf16[1024,4096]{1,0:T(8,128)(2,1)} %wout_hbm.1, ...), custom_call_target="tpu_custom_call" | custom-call | tf_op jit(solution)/shard_map/mixer/pallas_call | solution.py:402
  39.4 3.2 %finish.1 = bf16[512,4096]{1,0:T(8,128)(2,1)} custom-call(f32[512,4096]{1,0:T(8,128)S(1)} %get-tuple-element.8.acc, bf16[512,512]{1,0:T(8,128)(2,1)S(1)} %get-tuple-element.9.spec_b, bf16[512,4096]{1,0:T(8,128)(2,1)S(1)} %get-tuple-element.10.wmix_b), custom_call_target="tpu_custom_call" | custom-call | tf_op jit(solution)/shard_map/finish/pallas_call | solution.py:439
